TPU v7x, 32 devices: a whole 2x2x4 slice. The times are simulated.
32 devices in a mesh: grp: 2 (over x), ra: 4 (over z), cb: 4 (over y, core).
Axes of the slice: x: 2, y: 2, z: 4, core: 2. Of those that a mesh axis runs over, the one named last changes fastest.
Arguments:
- tokens: bfloat16 [256, 4096], P('grp', 'ra'), parts along dimension 0, may hold values from -30 to 30
- in_gain: float32 [4096], P('ra'), may hold values from 0.1 to 1.9
- gate_weight: float32 [4096, 11264], P('ra', 'cb'), may hold values from -0.09375 to 0.09375
- gate_scale: float32 [11264], P('cb'), may hold values from 0.3 to 3
- up_weight: float32 [4096, 11264], P('ra', 'cb'), may hold values from -0.09375 to 0.09375
- up_scale: float32 [11264], P('cb'), may hold values from 0.3 to 3
- down_weight: float32 [11264, 4096], P('cb', 'ra'), may hold values from -0.0546875 to 0.0546875
- down_scale: float32 [4096], P('ra'), may hold values from 0.3 to 3
- out_gain: float32 [4096], P('ra'), may hold values from 0.1 to 1.9
Outputs:
- result: bfloat16 [256, 4096], P('grp', 'ra'), parts along dimension 0
There are 2 independent parts, one for each index of `grp`. A program takes and returns all parts, laid end to end along the dimension named above; an argument that names none is the same for every part. Nothing has to cross between parts.
All inputs are finite; a program needn't handle non-finite values.
Results may differ from a plain program's by a relative error of at most 0.008.
Values may be sent and summed in bfloat16 or wider, within the bound.
A program may use at most 64 MiB of HBM per device.

v0:
```python
import jax
import jax.numpy as jnp
from jax import lax
from jax.sharding import PartitionSpec as P

EPSILON = 1e-06
RESIDUAL = 0.5


def local(
    tokens, in_gain, gate_weight, gate_scale, up_weight, up_scale, down_weight, down_scale, out_gain
):
    tok_float = tokens.astype(jnp.float32)
    local_squares = jnp.sum(tok_float * tok_float, axis=1)
    scaled = (tok_float * in_gain[None, :]).astype(jnp.bfloat16)
    gate_part = jnp.dot(
        scaled, gate_weight.astype(jnp.bfloat16), preferred_element_type=jnp.float32
    )
    up_part = jnp.dot(scaled, up_weight.astype(jnp.bfloat16), preferred_element_type=jnp.float32)
    features = tokens.shape[1] * lax.axis_size("ra")
    gate_sum, up_sum, share_squares = (
        lax.psum_scatter(gate_part, "ra", scatter_dimension=0, tiled=True),
        lax.psum_scatter(up_part, "ra", scatter_dimension=0, tiled=True),
        lax.psum_scatter(local_squares, "ra", scatter_dimension=0, tiled=True),
    )
    inv_rows = lax.rsqrt(share_squares / features + EPSILON)[:, None]
    gate_share = gate_sum * inv_rows * gate_scale[None, :]
    up_share = up_sum * inv_rows * up_scale[None, :]
    hidden_share = (jax.nn.silu(gate_share) * up_share).astype(jnp.bfloat16)
    hidden = lax.all_gather(hidden_share, "ra", axis=0, tiled=True)
    down_part = jnp.dot(
        hidden, down_weight.astype(jnp.bfloat16), preferred_element_type=jnp.float32
    )
    down_full = lax.psum(down_part, "cb")
    mixed_rows = RESIDUAL * tok_float + down_full * down_scale[None, :]
    out_total = lax.psum(jnp.sum(mixed_rows * mixed_rows, axis=1), "ra")
    inv_out = lax.rsqrt(out_total / features + EPSILON)[:, None]
    return (mixed_rows * inv_out * out_gain[None, :]).astype(jnp.bfloat16)


def solution(mesh):
    in_specs = (
        P("grp", "ra"),
        P("ra"),
        P("ra", "cb"),
        P("cb"),
        P("ra", "cb"),
        P("cb"),
        P("cb", "ra"),
        P("ra"),
        P("ra"),
    )
    out_specs = P("grp", "ra")
    return jax.shard_map(local, mesh=mesh, in_specs=in_specs, out_specs=out_specs, check_vma=False)
```

profile of v0, /device:TPU:0, one launch (start us, length us, event | category | flops | bytes accessed | tf_op | source)
XLA Modules:
  0.0 162.6 jit_solution(1008541971637551343)
XLA Ops:
  6.5 0.0 copy-start.1
  6.5 0.0 reduce-scatter.3.cloned.1.call-start
  6.5 6.5 %fusion.4 = f32[128,2816]{1,0:T(8,128)} fusion(f32[1024,2816]{1,0:T(8,128)} %param.11, bf16[128,1024]{1,0:T(8,128)(2,1)} %param.9, f32[1024]{0:T(1024)} %param.10), kind=kOutput, calls=%fused_computation.4 | convolution fusion | flops 741474304 | bytes 13242368 | tf_op jit(solution)/shard_map/dot_general | solution.py:16
  13.0 0.0 reduce-scatter.3.cloned.1.call-update
  13.0 0.0 copy-start.6
  13.1 0.0 copy-start.3
  13.1 0.0 copy-start.4
  13.1 0.0 reduce-scatter.5.cloned.1.call-start
  13.1 0.0 copy-done.1
  13.1 0.0 copy-done
  13.1 6.3 %fusion.2 = f32[128,2816]{1,0:T(8,128)} fusion(f32[1024,2816]{1,0:T(8,128)} %param.13, bf16[128,1024]{1,0:T(8,128)(2,1)S(1)} %copy-done, f32[1024]{0:T(1024)S(1)} %copy-done.1), kind=kOutput, calls=%fused_computation.2 | convolution fusion | flops 741474304 | bytes 13242368 | tf_op jit(solution)/shard_map/dot_general | solution.py:19
  19.5 0.0 reduce-scatter.5.cloned.1.call-update
  19.5 0.0 all-reduce.3.cloned.1.call-start
  19.5 0.0 copy-done.6
  19.5 0.6 dynamic-slice
  20.8 0.1 fusion.8
  20.9 14.0 %all-reduce = f32[128]{0:T(128)S(1)} all-reduce(f32[128]{0:T(128)S(1)} %fusion.8), channel_id=3, replica_groups=mesh['grp'=2,'ra'=4,'cb'=4] {'ra'}, use_global_device_ids=true, to_apply=%region_2.0.clone | all-reduce | flops 128 | bytes 1024
  34.9 0.1 fusion.12
  35.0 14.6 %reduce-scatter.3.cloned.1.call-done = f32[32,2816]{1,0:T(8,128)} async-done(((f32[128,2816]{1,0:T(8,128)}), f32[32,2816]{1,0:T(8,128)}) %reduce-scatter.3.cloned.1.call-update) | async-done | bytes 360464 | tf_op jit(solution)/shard_map/reduce_scatter | solution.py:22
  49.6 34.5 %reduce-scatter.5.cloned.1.call-done = f32[32,2816]{1,0:T(8,128)} async-done(((f32[128,2816]{1,0:T(8,128)}), f32[32,2816]{1,0:T(8,128)}) %reduce-scatter.5.cloned.1.call-update) | async-done | bytes 360464 | tf_op jit(solution)/shard_map/reduce_scatter | solution.py:23
  84.1 0.0 copy-done.3
  84.1 0.0 copy-done.4
  84.1 1.3 multiply_convert_fusion.1
  85.4 17.2 %all_gather.3 = bf16[128,2816]{1,0:T(8,128)(2,1)S(1)} all-gather(bf16[32,2816]{1,0:T(8,128)(2,1)S(1)} %multiply_convert_fusion.1), channel_id=1, replica_groups=mesh['grp'=2,'ra'=4,'cb'=4] {'ra'}, dimensions={0}, use_global_device_ids=true | all-gather | bytes 901120 | tf_op jit(solution)/shard_map/all_gather | solution.py:30
  102.6 6.0 %fusion = f32[128,1024]{1,0:T(8,128)} fusion(bf16[128,2816]{1,0:T(8,128)(2,1)S(1)} %all_gather.3, f32[2816,1024]{1,0:T(8,128)} %param.15), kind=kOutput, calls=%fused_computation | convolution fusion | flops 741081088 | bytes 12779520 | tf_op jit(solution)/shard_map/dot_general | solution.py:31
  108.7 0.0 all-reduce.3.cloned.1.call-update
  108.7 32.6 %all-reduce.3.cloned.1.call-done = f32[128,1024]{1,0:T(8,128)} async-done(((f32[128,1024]{1,0:T(8,128)}), f32[128,1024]{1,0:T(8,128)}) %all-reduce.3.cloned.1.call-update) | async-done | bytes 524304 | tf_op jit(solution)/shard_map/psum | solution.py:34
  141.3 0.0 copy-done.2
  141.3 1.2 multiply_reduce_fusion
  142.5 11.7 %psum.15 = f32[128]{0:T(128)S(1)} all-reduce(f32[128]{0:T(128)S(1)} %multiply_reduce_fusion), channel_id=1, replica_groups=mesh['grp'=2,'ra'=4,'cb'=4] {'ra'}, use_global_device_ids=true, to_apply=%region_6.7 | all-reduce | flops 128 | bytes 1024 | tf_op jit(solution)/shard_map/psum | solution.py:36
  154.2 0.0 copy-done.5
  154.2 1.9 %multiply_convert_fusion = bf16[128,1024]{1,0:T(8,128)(2,1)} fusion(f32[128,1024]{1,0:T(8,128)} %all-reduce.3.cloned.1.call-done, bf16[128,1024]{1,0:T(8,128)(2,1)S(1)} %copy-done, f32[1024]{0:T(1024)S(1)} %copy-done.5, f32[128]{0:T(128)S(1)} %add_rsqrt_fusion, f32[1024]{0:T(1024)S(1)} %copy-done.2), kind=kLoop, calls=%fused_computation.12 | loop fusion | flops 917504 | bytes 1057280 | tf_op jit(solution)/shard_map/convert_element_type | solution.py:38
  (4 shorter events, 0.0 us)
Async XLA Ops:
  6.5 6.6 %copy-start.1 = (f32[1024]{0:T(1024)S(1)}, f32[1024]{0:T(1024)}, u32[]{:S(2)}) copy-start(f32[1024]{0:T(1024)} %param.10) | copy-start | bytes 12292
  6.5 6.6 %copy-start = (bf16[128,1024]{1,0:T(8,128)(2,1)S(1)}, bf16[128,1024]{1,0:T(8,128)(2,1)}, u32[]{:S(2)}) copy-start(bf16[128,1024]{1,0:T(8,128)(2,1)} %param.9) | copy-start | bytes 786436
  6.5 43.0 %reduce-scatter.3.cloned.1.call-start = ((), (), s32[]{:S(2)}) async-start(), calls=%async_computation.2 | async-start | bytes 1802240 | tf_op jit(solution)/shard_map/reduce_scatter | solution.py:22
  13.0 6.5 %copy-start.6 = (u32[32]{0:T(128)S(1)}, u32[32]{0:T(128)}, u32[]{:S(2)}) copy-start(u32[32]{0:T(128)} %constant.17) | copy-start | bytes 388
  13.1 71.1 %copy-start.3 = (f32[2816]{0:T(1024)S(1)}, f32[2816]{0:T(1024)}, u32[]{:S(2)}) copy-start(f32[2816]{0:T(1024)} %param.14) | copy-start | bytes 33796
  13.1 71.1 %copy-start.4 = (f32[2816]{0:T(1024)S(1)}, f32[2816]{0:T(1024)}, u32[]{:S(2)}) copy-start(f32[2816]{0:T(1024)} %param.12) | copy-start | bytes 33796
  13.1 71.0 %reduce-scatter.5.cloned.1.call-start = ((), (), s32[]{:S(2)}) async-start(), calls=%async_computation.3 | async-start | bytes 1802240 | tf_op jit(solution)/shard_map/reduce_scatter | solution.py:23
  19.5 121.8 %all-reduce.3.cloned.1.call-start = ((), (), s32[]{:S(2)}) async-start(), calls=%async_computation.4 | async-start | bytes 1048576 | tf_op jit(solution)/shard_map/psum | solution.py:34
  102.6 38.6 %copy-start.2 = (f32[1024]{0:T(1024)S(1)}, f32[1024]{0:T(1024)}, u32[]{:S(2)}) copy-start(f32[1024]{0:T(1024)} %param.16) | copy-start | bytes 12292
  102.6 51.5 %copy-start.5 = (f32[1024]{0:T(1024)S(1)}, f32[1024]{0:T(1024)}, u32[]{:S(2)}) copy-start(f32[1024]{0:T(1024)} %param.17) | copy-start | bytes 12292
Sparse Core Ops, SparseCore 0:
  13.2 36.3 reduce-scatter.2
  51.9 32.1 reduce-scatter.4
  108.8 32.3 all-reduce.2
where the time goes:
time: 163 us
  waiting for transfers between devices  81.7 us (50%)
  blocking collectives  42.9 us (26%)
  matrix products  18.8 us (12%)
  between operations  13.8 us (8%)
  other arithmetic  4.61 us (3%)
    reduce_scatter x1, waiting for transfers between devices, local(): lax.psum_scatter(up_part, 'ra', scatter_dimension=0, tiled=True)  34.5 us
    psum x1, waiting for transfers between devices, local(): down_full = lax.psum(down_part, 'cb')  32.6 us
    all_gather x1, blocking collectives, local(): hidden = lax.all_gather(hidden_share, 'ra', axis=0, tiled=True)  17.2 us
    reduce_scatter x1, waiting for transfers between devices, local(): lax.psum_scatter(gate_part, 'ra', scatter_dimension=0, tiled=True)  14.6 us
    unnamed x1, blocking collectives  14 us
    psum x1, blocking collectives, local(): out_total = lax.psum(jnp.sum(mixed_rows * mixed_rows, axis=1), 'ra')  11.7 us
    dot_general x1, matrix products, local(): jnp.dot(scaled, gate_weight.astype(jnp.bfloat16), preferred_element_type=...  6.47 us
    dot_general x1, matrix products, local(): jnp.dot(scaled, up_weight.astype(jnp.bfloat16), preferred_element_type=jn...  6.31 us
  transfers between devices with their start and end apart: 3, of which 3 were waited for; matrix products, arithmetic and copies ran while one was open for 4% of the time, Pallas kernels for 0%

commit v1 on v0

--- a/solution.py
+++ b/solution.py
@@ -1,6 +1,9 @@
+import functools
 import jax
 import jax.numpy as jnp
 from jax import lax
+from jax.experimental import pallas as pl
+from jax.experimental.pallas import tpu as pltpu
 from jax.sharding import PartitionSpec as P
 
 EPSILON = 1e-06
@@ -36,6 +39,296 @@
     out_total = lax.psum(jnp.sum(mixed_rows * mixed_rows, axis=1), "ra")
     inv_out = lax.rsqrt(out_total / features + EPSILON)[:, None]
     return (mixed_rows * inv_out * out_gain[None, :]).astype(jnp.bfloat16)
+
+
+MESH = pl.DeviceIdType.MESH
+WIDTH = 256
+LAG = 2
+
+
+def kernel(
+    n,
+    tok_hbm, gain_hbm, gate_hbm, gscale_hbm, up_hbm, uscale_hbm, down_hbm, dscale_hbm, ogain_hbm,
+    out_ref,
+    tok, gain, gate, gscale, up, uscale, down, dscale, ogain,
+    scaled, part, sent, got, hidden, acc, spread, sq_own, sq_got, inv, half_sent, half_got,
+    y_sent, y_got, mixed, out_own, out_got,
+    small_sem, gate_sem, up_sem, down_sem, rs_send, rs_recv, ag_send, ag_recv,
+    sq_send, sq_recv, half_sem, y_sem, mix_sem, out_send, out_recv,
+):
+    chunks, half = gate.shape[0], tok.shape[0] // 2
+    rows = 2 * half
+    features = tok.shape[1] * n
+    z, cb = lax.axis_index("ra"), lax.axis_index("cb")
+    core = lax.rem(cb, 2)
+    mate = cb + 1 - 2 * core
+    across = lax.rem(cb + 2, 4)
+    right, left = lax.rem(z + 1, n), lax.rem(z + n - 1, n)
+
+    smalls = [
+        pltpu.make_async_copy(src, dst, small_sem.at[i])
+        for i, (src, dst) in enumerate([
+            (tok_hbm, tok), (gain_hbm, gain), (gscale_hbm, gscale),
+            (uscale_hbm, uscale), (dscale_hbm, dscale), (ogain_hbm, ogain),
+        ])
+    ]
+
+    def gate_copy(j):
+        cols = pl.ds(pl.multiple_of(j * WIDTH, WIDTH), WIDTH)
+        return pltpu.make_async_copy(gate_hbm.at[:, cols], gate.at[j], gate_sem.at[j])
+
+    def up_copy(j):
+        cols = pl.ds(pl.multiple_of(j * WIDTH, WIDTH), WIDTH)
+        return pltpu.make_async_copy(up_hbm.at[:, cols], up.at[j], up_sem.at[j])
+
+    def down_copy(j):
+        at = pl.ds(pl.multiple_of(j * WIDTH, WIDTH), WIDTH)
+        return pltpu.make_async_copy(down_hbm.at[at, :], down.at[j], down_sem.at[j])
+
+    for copy in smalls:
+        copy.start()
+    for j in range(chunks):
+        gate_copy(j).start()
+        up_copy(j).start()
+    for j in range(chunks):
+        down_copy(j).start()
+
+    barrier = pltpu.get_barrier_semaphore()
+    for step in range(1, n):
+        for who in (cb, mate):
+            pl.semaphore_signal(barrier, inc=1, device_id={"ra": lax.rem(z + step, n), "cb": who}, device_id_type=MESH)
+    for who in (mate, across):
+        pl.semaphore_signal(barrier, inc=1, device_id={"cb": who}, device_id_type=MESH)
+
+    for copy in smalls:
+        copy.wait()
+    tok_float = tok[...].astype(jnp.float32)
+    scaled[...] = (tok_float * gain[...]).astype(jnp.bfloat16)
+    squares = jnp.sum(tok_float * tok_float, axis=1, keepdims=True)
+    spread[...] = jnp.broadcast_to(squares, (rows, 128))
+    sq_own[0] = spread[...].T[:8]
+
+    pl.semaphore_wait(barrier, 2 * (n - 1) + 2)
+
+    def sq_copy(step, goal):
+        return pltpu.make_async_remote_copy(
+            sq_own.at[0], sq_got.at[step - 1], sq_send.at[goal], sq_recv.at[step - 1],
+            device_id={"ra": lax.rem(z + step, n)}, device_id_type=MESH,
+        )
+
+    for goal, end in enumerate((0, n - 1)):
+        for step in range(1, n):
+            @pl.when(lax.rem(z + step, n) == end)
+            def _():
+                sq_copy(step, goal).start()
+
+    def rs_copy(j, side):
+        return pltpu.make_async_remote_copy(
+            sent.at[side, j], got.at[side, j], rs_send.at[side, j], rs_recv.at[side, j],
+            device_id={"ra": right if side else left}, device_id_type=MESH,
+        )
+
+    def ag_copy(j, side):
+        ref = hidden.at[j, pl.ds(side * half, half)]
+        return pltpu.make_async_remote_copy(
+            ref, ref, ag_send.at[side, j], ag_recv.at[side, j],
+            device_id={"ra": left if side else right}, device_id_type=MESH,
+        )
+
+    def rs_step(t, side):
+        place = z if side else n - 1 - z
+        j = t - LAG * place
+        own = pl.ds(side * half, half)
+
+        @pl.when((j >= 0) & (j < chunks))
+        def _():
+            @pl.when(place == 0)
+            def _():
+                sent[side, j] = part[j, own].astype(jnp.bfloat16)
+                rs_copy(j, side).start()
+
+            @pl.when((place > 0) & (place < n - 1))
+            def _():
+                rs_copy(j, side).wait_recv()
+                sent[side, j] = (part[j, own] + got[side, j].astype(jnp.float32)).astype(jnp.bfloat16)
+                rs_copy(j, side).start()
+
+            @pl.when(place == n - 1)
+            def _():
+                @pl.when(j == 0)
+                def _():
+                    for step in range(1, n):
+                        sq_copy(step, 0).wait_recv()
+                    total = sq_own[0] + sq_got[0]
+                    for step in range(2, n):
+                        total = total + sq_got[step - 1]
+                    spread[...] = jnp.broadcast_to(total[:1], (128, 128)).T
+                    inv[...] = lax.rsqrt(spread[...] / features + EPSILON)
+
+                rs_copy(j, side).wait_recv()
+                cols = pl.ds(pl.multiple_of(j * WIDTH, WIDTH), WIDTH)
+                scale = inv[own][:, :1]
+                total = part[j, own] + got[side, j].astype(jnp.float32)
+                gate_share = total[:, :WIDTH] * scale * gscale[:, cols]
+                up_share = total[:, WIDTH:] * scale * uscale[:, cols]
+                hidden[j, own] = (jax.nn.silu(gate_share) * up_share).astype(jnp.bfloat16)
+                ag_copy(j, side).start()
+
+    def rs_loop(t, carry):
+        @pl.when(t < chunks)
+        def _():
+            gate_copy(t).wait()
+            part[t, :, :WIDTH] = jnp.dot(scaled[...], gate[t].astype(jnp.bfloat16), preferred_element_type=jnp.float32)
+            up_copy(t).wait()
+            part[t, :, WIDTH:] = jnp.dot(scaled[...], up[t].astype(jnp.bfloat16), preferred_element_type=jnp.float32)
+
+        rs_step(t, 0)
+        rs_step(t, 1)
+        return carry
+
+    lax.fori_loop(0, chunks + LAG * (n - 1), rs_loop, 0)
+
+    def ag_step(u, side):
+        place = n - 1 - z if side else z
+        j = u - LAG * (place - 1)
+
+        @pl.when((place > 0) & (j >= 0) & (j < chunks))
+        def _():
+            ag_copy(j, side).wait_recv()
+
+            @pl.when(place < n - 1)
+            def _():
+                ag_copy(j, side).start()
+
+    acc[...] = jnp.zeros_like(acc)
+
+    def ag_loop(u, carry):
+        ag_step(u, 0)
+        ag_step(u, 1)
+        j = u - LAG * (lax.max(z, n - 1 - z) - 1)
+
+        @pl.when((j >= 0) & (j < chunks))
+        def _():
+            down_copy(j).wait()
+            acc[...] += jnp.dot(hidden[j], down[j].astype(jnp.bfloat16), preferred_element_type=jnp.float32)
+
+        return carry
+
+    lax.fori_loop(0, chunks + LAG * (n - 2), ag_loop, 0)
+
+    mine = pl.ds(pl.multiple_of(core * half, half), half)
+    theirs = pl.ds(pl.multiple_of((1 - core) * half, half), half)
+    half_sent[...] = acc[theirs].astype(jnp.bfloat16)
+    half_copy = pltpu.make_async_remote_copy(
+        half_sent, half_got, half_sem.at[0], half_sem.at[1], device_id={"cb": mate}, device_id_type=MESH
+    )
+    half_copy.start()
+    half_copy.wait()
+    y_sent[...] = (acc[mine] + half_got[...].astype(jnp.float32)).astype(jnp.bfloat16)
+    y_copy = pltpu.make_async_remote_copy(
+        y_sent, y_got, y_sem.at[0], y_sem.at[1], device_id={"cb": across}, device_id_type=MESH
+    )
+    y_copy.start()
+    y_copy.wait()
+    summed = y_sent[...].astype(jnp.float32) + y_got[...].astype(jnp.float32)
+    mixed[0] = RESIDUAL * tok[mine].astype(jnp.float32) + summed * dscale[...]
+    mix_copy = pltpu.make_async_remote_copy(
+        mixed.at[0], mixed.at[1], mix_sem.at[0], mix_sem.at[1], device_id={"cb": mate}, device_id_type=MESH
+    )
+    mix_copy.start()
+    squares = jnp.sum(mixed[0] * mixed[0], axis=1, keepdims=True)
+    spread[...] = jnp.zeros_like(spread)
+    spread[mine] = jnp.broadcast_to(squares, (half, 128))
+    out_own[...] = spread[...].T[:8]
+
+    def out_copies():
+        made = []
+        for step in range(n):
+            for other in range(2):
+                if step or other:
+                    at = 2 * step + other - 1
+                    made.append(pltpu.make_async_remote_copy(
+                        out_own, out_got.at[at], out_send.at[at], out_recv.at[at],
+                        device_id={"ra": lax.rem(z + step, n), "cb": mate if other else cb},
+                        device_id_type=MESH,
+                    ))
+        return made
+
+    for copy in out_copies():
+        copy.start()
+    for copy in out_copies():
+        copy.wait_recv()
+    total = out_own[...]
+    for at in range(2 * n - 1):
+        total = total + out_got[at]
+    spread[...] = jnp.broadcast_to(total[:1], (128, 128)).T
+    spread[...] = lax.rsqrt(spread[...] / features + EPSILON)
+    out_ref[mine] = (mixed[0] * spread[mine][:, :1] * ogain[...]).astype(jnp.bfloat16)
+    mix_copy.wait()
+    out_ref[theirs] = (mixed[1] * spread[theirs][:, :1] * ogain[...]).astype(jnp.bfloat16)
+
+    for copy in out_copies():
+        copy.wait_send()
+    for goal, end in enumerate((0, n - 1)):
+        @pl.when(z != end)
+        def _():
+            sq_copy(1, goal).wait_send()
+
+    def drain(j, carry):
+        @pl.when(z > 0)
+        def _():
+            rs_copy(j, 0).wait_send()
+            ag_copy(j, 1).wait_send()
+
+        @pl.when(z < n - 1)
+        def _():
+            rs_copy(j, 1).wait_send()
+            ag_copy(j, 0).wait_send()
+
+        return carry
+
+    lax.fori_loop(0, chunks, drain, 0)
+
+
+def fused(
+    tokens, in_gain, gate_weight, gate_scale, up_weight, up_scale, down_weight, down_scale, out_gain
+):
+    n = lax.axis_size("ra")
+    rows, depth = tokens.shape
+    units, width = down_weight.shape
+    half, chunks = rows // 2, units // WIDTH
+    f32, bf16 = jnp.float32, jnp.bfloat16
+    vmem, dma = pltpu.VMEM, pltpu.SemaphoreType.DMA
+    return pl.pallas_call(
+        functools.partial(kernel, n),
+        out_shape=jax.ShapeDtypeStruct((rows, width), bf16),
+        in_specs=[pl.BlockSpec(memory_space=pl.ANY)] * 9,
+        out_specs=pl.BlockSpec(memory_space=pltpu.VMEM),
+        scratch_shapes=[
+            vmem((rows, depth), bf16), vmem((1, depth), f32),
+            vmem((chunks, depth, WIDTH), f32), vmem((1, units), f32),
+            vmem((chunks, depth, WIDTH), f32), vmem((1, units), f32),
+            vmem((chunks, WIDTH, width), f32), vmem((1, width), f32), vmem((1, width), f32),
+            vmem((rows, depth), bf16), vmem((chunks, rows, 2 * WIDTH), f32),
+            vmem((2, chunks, half, 2 * WIDTH), bf16), vmem((2, chunks, half, 2 * WIDTH), bf16),
+            vmem((chunks, rows, WIDTH), bf16), vmem((rows, width), f32),
+            vmem((rows, 128), f32), vmem((1, 8, 128), f32), vmem((n - 1, 8, 128), f32),
+            vmem((rows, 128), f32), vmem((half, width), bf16), vmem((half, width), bf16),
+            vmem((half, width), bf16), vmem((half, width), bf16), vmem((2, half, width), f32),
+            vmem((8, 128), f32), vmem((2 * n - 1, 8, 128), f32),
+            dma((6,)), dma((chunks,)), dma((chunks,)), dma((chunks,)),
+            dma((2, chunks)), dma((2, chunks)), dma((2, chunks)), dma((2, chunks)),
+            dma((2,)), dma((n - 1,)), dma((2,)), dma((2,)), dma((2,)),
+            dma((2 * n - 1,)), dma((2 * n - 1,)),
+        ],
+        compiler_params=pltpu.CompilerParams(
+            collective_id=0, has_side_effects=True, vmem_limit_bytes=60 * 2**20
+        ),
+        name="fused_ffn",
+    )(
+        tokens, in_gain.reshape(1, -1), gate_weight, gate_scale.reshape(1, -1), up_weight,
+        up_scale.reshape(1, -1), down_weight, down_scale.reshape(1, -1), out_gain.reshape(1, -1),
+    )
 
 
 def solution(mesh):
@@ -51,4 +344,5 @@
         P("ra"),
     )
     out_specs = P("grp", "ra")
-    return jax.shard_map(local, mesh=mesh, in_specs=in_specs, out_specs=out_specs, check_vma=False)
+    body = fused if mesh.shape["ra"] == 4 and mesh.shape["cb"] == 4 else local
+    return jax.shard_map(body, mesh=mesh, in_specs=in_specs, out_specs=out_specs, check_vma=False)

time: 163 us -> 75.6 us (0.46)
  waiting for transfers between devices: 81.7 us -> 0 us
  Pallas kernels: 0 us -> 71 us
  blocking collectives: 42.9 us -> 0 us
  matrix products: 18.8 us -> 0 us
  between operations: 13.8 us -> 0.01 us
  other arithmetic: 4.61 us -> 0 us
  local copies, waits for them, and re-layouts: 0.62 us -> 4.29 us
    pallas_call x0 -> x1, Pallas kernels: none -> 71 us  [fused(): pl.pallas_call(functools.partial(kernel, n), out_shape=jax.ShapeDtypeStru...]
    reduce_scatter x2 -> x0, waiting for transfers between devices: 49.1 us -> none  [the longest x1 34.5 us: local(): lax.psum_scatter(up_part, 'ra', scatter_dimension=0, tiled=True)]
    psum x1 -> x0, waiting for transfers between devices: 32.6 us -> none  [local(): down_full = lax.psum(down_part, 'cb')]
    dot_general x3 -> x0, matrix products: 18.8 us -> none  [the longest x1 6.47 us: local(): jnp.dot(scaled, gate_weight.astype(jnp.bfloat16), preferred_element_type=...]
    all_gather x1 -> x0, blocking collectives: 17.2 us -> none  [local(): hidden = lax.all_gather(hidden_share, 'ra', axis=0, tiled=True)]
    unnamed x1 -> x0, blocking collectives: 14 us -> none
    psum x1 -> x0, blocking collectives: 11.7 us -> none  [local(): out_total = lax.psum(jnp.sum(mixed_rows * mixed_rows, axis=1), 'ra')]
    convert_element_type x2 -> x0, other arithmetic: 3.16 us -> none  [the longest x1 1.87 us: local(): return (mixed_rows * inv_out * out_gain[None, :]).astype(jnp.bfloat16)]
  transfers between devices with their start and end apart: 3 -> 0, of which waited for: 3 -> 0; matrix products, arithmetic and copies ran while one was open for 4% -> 0% of each run, Pallas kernels for 0% -> 0%
where the time goes in v1:
time: 75.6 us; the launch traced here: 75.3 us
  Pallas kernels  71 us (94%)
  local copies, waits for them, and re-layouts  4.29 us (6%)
    pallas_call x1, Pallas kernels, fused(): pl.pallas_call(functools.partial(kernel, n), out_shape=jax.ShapeDtypeStru...  71 us
    unnamed x1, local copies, waits for them, and re-layouts  1.67 us

profile of v1, /device:TPU:0, one launch (start us, length us, event | category | flops | bytes accessed | tf_op | source)
XLA Modules:
  0.0 75.3 jit_solution(3802076875815116785)
XLA Ops:
  0.0 1.3 %reshape.16.gscale_hbm = f32[1,2816]{1,0:T(1,128)} reshape(f32[2816]{0:T(1024)} %param.12) | data formatting | bytes 22528 | tf_op jit(solution)/shard_map/reshape | solution.py:329
  1.3 1.3 %reshape.17.uscale_hbm = f32[1,2816]{1,0:T(1,128)} reshape(f32[2816]{0:T(1024)} %param.14) | data formatting | bytes 22528 | tf_op jit(solution)/shard_map/reshape | solution.py:330
  2.6 71.0 %fused_ffn.1 = bf16[128,1024]{1,0:T(8,128)(2,1)} custom-call(bf16[128,1024]{1,0:T(8,128)(2,1)} %tok_hbm.1, f32[1,1024]{1,0:T(1,128)} %bitcast.3, f32[1024,2816]{1,0:T(8,128)} %gate_hbm.1, f32[1,2816]{1,0:T(1,128)} %reshape.16.gscale_hbm, f32[1024,2816]{1,0:T(8,128)} %up_hbm.1, f32[1,2816]{1,0:T(1,128)} %reshape.17.uscale_hbm, f32[2816,1024]{1,0:T(8,128)} %down_hbm.1, ...), custom_call_target="tpu_custom_call" | custom-call | tf_op jit(solution)/shard_map/fused_ffn/pallas_call | solution.py:302
  73.6 1.7 %copy.11 = bf16[128,1024]{1,0:T(8,128)(2,1)} copy(bf16[128,1024]{1,0:T(8,128)(2,1)} %fused_ffn.1) | data formatting | bytes 524288

commit v2 on v1

--- a/solution.py
+++ b/solution.py
@@ -43,7 +43,9 @@
 
 MESH = pl.DeviceIdType.MESH
 WIDTH = 256
-LAG = 2
+RS_LAG = 3
+AG_LAG = 5
+AHEAD = 3
 
 
 def kernel(
@@ -87,11 +89,9 @@
 
     for copy in smalls:
         copy.start()
-    for j in range(chunks):
+    for j in range(min(AHEAD, chunks)):
         gate_copy(j).start()
         up_copy(j).start()
-    for j in range(chunks):
-        down_copy(j).start()
 
     barrier = pltpu.get_barrier_semaphore()
     for step in range(1, n):
@@ -137,7 +137,7 @@
 
     def rs_step(t, side):
         place = z if side else n - 1 - z
-        j = t - LAG * place
+        j = t - RS_LAG * place
         own = pl.ds(side * half, half)
 
         @pl.when((j >= 0) & (j < chunks))
@@ -166,12 +166,14 @@
                     inv[...] = lax.rsqrt(spread[...] / features + EPSILON)
 
                 rs_copy(j, side).wait_recv()
-                cols = pl.ds(pl.multiple_of(j * WIDTH, WIDTH), WIDTH)
-                scale = inv[own][:, :1]
+                scale = inv[own]
                 total = part[j, own] + got[side, j].astype(jnp.float32)
-                gate_share = total[:, :WIDTH] * scale * gscale[:, cols]
-                up_share = total[:, WIDTH:] * scale * uscale[:, cols]
-                hidden[j, own] = (jax.nn.silu(gate_share) * up_share).astype(jnp.bfloat16)
+                tiles = WIDTH // 128
+                for i in range(tiles):
+                    at, cols = pl.ds(j * tiles + i, 1), slice(128 * i, 128 * (i + 1))
+                    gate_share = total[:, cols] * scale * gscale[at]
+                    up_share = total[:, WIDTH:][:, cols] * scale * uscale[at]
+                    hidden[j, own, cols] = (jax.nn.silu(gate_share) * up_share).astype(jnp.bfloat16)
                 ag_copy(j, side).start()
 
     def rs_loop(t, carry):
@@ -180,17 +182,28 @@
             gate_copy(t).wait()
             part[t, :, :WIDTH] = jnp.dot(scaled[...], gate[t].astype(jnp.bfloat16), preferred_element_type=jnp.float32)
             up_copy(t).wait()
+
+            @pl.when(t + AHEAD < chunks)
+            def _():
+                gate_copy(t + AHEAD).start()
+                up_copy(t + AHEAD).start()
+
+            @pl.when(t == chunks - 1)
+            def _():
+                for j in range(chunks):
+                    down_copy(j).start()
+
             part[t, :, WIDTH:] = jnp.dot(scaled[...], up[t].astype(jnp.bfloat16), preferred_element_type=jnp.float32)
 
         rs_step(t, 0)
         rs_step(t, 1)
         return carry
 
-    lax.fori_loop(0, chunks + LAG * (n - 1), rs_loop, 0)
+    lax.fori_loop(0, chunks + RS_LAG * (n - 1), rs_loop, 0)
 
     def ag_step(u, side):
         place = n - 1 - z if side else z
-        j = u - LAG * (place - 1)
+        j = u - AG_LAG * (place - 1)
 
         @pl.when((place > 0) & (j >= 0) & (j < chunks))
         def _():
@@ -205,7 +218,7 @@
     def ag_loop(u, carry):
         ag_step(u, 0)
         ag_step(u, 1)
-        j = u - LAG * (lax.max(z, n - 1 - z) - 1)
+        j = u - AG_LAG * (lax.max(z, n - 1 - z) - 1)
 
         @pl.when((j >= 0) & (j < chunks))
         def _():
@@ -214,7 +227,7 @@
 
         return carry
 
-    lax.fori_loop(0, chunks + LAG * (n - 2), ag_loop, 0)
+    lax.fori_loop(0, chunks + AG_LAG * (n - 2), ag_loop, 0)
 
     mine = pl.ds(pl.multiple_of(core * half, half), half)
     theirs = pl.ds(pl.multiple_of((1 - core) * half, half), half)
@@ -306,8 +319,8 @@
         out_specs=pl.BlockSpec(memory_space=pltpu.VMEM),
         scratch_shapes=[
             vmem((rows, depth), bf16), vmem((1, depth), f32),
-            vmem((chunks, depth, WIDTH), f32), vmem((1, units), f32),
-            vmem((chunks, depth, WIDTH), f32), vmem((1, units), f32),
+            vmem((chunks, depth, WIDTH), f32), vmem((units // 128, 128), f32),
+            vmem((chunks, depth, WIDTH), f32), vmem((units // 128, 128), f32),
             vmem((chunks, WIDTH, width), f32), vmem((1, width), f32), vmem((1, width), f32),
             vmem((rows, depth), bf16), vmem((chunks, rows, 2 * WIDTH), f32),
             vmem((2, chunks, half, 2 * WIDTH), bf16), vmem((2, chunks, half, 2 * WIDTH), bf16),
@@ -326,8 +339,8 @@
         ),
         name="fused_ffn",
     )(
-        tokens, in_gain.reshape(1, -1), gate_weight, gate_scale.reshape(1, -1), up_weight,
-        up_scale.reshape(1, -1), down_weight, down_scale.reshape(1, -1), out_gain.reshape(1, -1),
+        tokens, in_gain.reshape(1, -1), gate_weight, gate_scale.reshape(-1, 128), up_weight,
+        up_scale.reshape(-1, 128), down_weight, down_scale.reshape(1, -1), out_gain.reshape(1, -1),
     )
 
 

time: 75.6 us -> 55.3 us (0.73)
  Pallas kernels: 71 us -> 53.5 us
  local copies, waits for them, and re-layouts: 4.29 us -> 1.67 us
    pallas_call x1, Pallas kernels: 71 us -> 53.5 us  [fused(): pl.pallas_call(functools.partial(kernel, n), out_shape=jax.ShapeDtypeStru...]
    reshape x2 -> x0, local copies, waits for them, and re-layouts: 2.62 us -> none  [the longest x1 1.31 us: fused(): gate_scale.reshape(1, -1)]
where the time goes in v2:
time: 55.3 us; the launch traced here: 55.1 us
  Pallas kernels  53.5 us (97%)
  local copies, waits for them, and re-layouts  1.67 us (3%)
    pallas_call x1, Pallas kernels, fused(): pl.pallas_call(functools.partial(kernel, n), out_shape=jax.ShapeDtypeStru...  53.5 us
    unnamed x1, local copies, waits for them, and re-layouts  1.67 us

profile of v2, /device:TPU:0, one launch (start us, length us, event | category | flops | bytes accessed | tf_op | source)
XLA Modules:
  0.0 55.1 jit_solution(12540979206602697261)
XLA Ops:
  0.0 53.5 %fused_ffn.1 = bf16[128,1024]{1,0:T(8,128)(2,1)} custom-call(bf16[128,1024]{1,0:T(8,128)(2,1)} %tok_hbm.1, f32[1,1024]{1,0:T(1,128)} %bitcast.7, f32[1024,2816]{1,0:T(8,128)} %gate_hbm.1, f32[22,128]{1,0:T(8,128)} %bitcast.5, f32[1024,2816]{1,0:T(8,128)} %up_hbm.1, f32[22,128]{1,0:T(8,128)} %bitcast.6, f32[2816,1024]{1,0:T(8,128)} %down_hbm.1, ...), custom_call_target="tpu_custom_call" | custom-call | tf_op jit(solution)/shard_map/fused_ffn/pallas_call | solution.py:315
  53.5 1.7 %copy.11 = bf16[128,1024]{1,0:T(8,128)(2,1)} copy(bf16[128,1024]{1,0:T(8,128)(2,1)} %fused_ffn.1) | data formatting | bytes 524288
